TPU v7x, 32 devices: a whole 2x2x4 slice. The times are simulated.
32 devices in a mesh: sp: 16 (over z, y, x), tp: 2 (over core).
Axes of the slice: x: 2, y: 2, z: 4, core: 2. Of those that a mesh axis runs over, the one named last changes fastest.
Arguments:
- skip_path_inputs: bfloat16 [2048, 2048], P('sp'), may hold values from -62 to 62
- probe_vectors: bfloat16 [2048, 1024], P('sp', 'tp'), may hold values from -6 to 6
- lookup_vectors: bfloat16 [2048, 1024], P('sp', 'tp'), may hold values from -6 to 6
- payload_vectors: bfloat16 [2048, 1024], P('sp', 'tp'), may hold values from -6 to 6
- learning_strength_preacts: float32 [2, 2048, 8], P(None, 'sp', 'tp'), may hold values from -6 to 6
- forget_preacts: float32 [2, 2048, 8], P(None, 'sp', 'tp'), may hold values from -5 to 5
- forgetting_speed_exponent: float32 [2, 8], P(None, 'tp'), may hold values from -12 to -2
- extra_forgetting_spikes: float32 [2, 2048, 8], P(None, 'sp', 'tp'), may hold values from -0.7 to 0
- sample_membership: int32 [2048], P('sp'), may hold values from 0 to 3, never falling along the last dimension, each value on 1 to 1024 neighbouring positions
- channel_group_scaling: float32 [128], replicated, may hold values from 0.1 to 1.9
- blend_exit_weights: bfloat16 [1024, 2048], P('tp'), may hold values from -0.1875 to 0.1875
- dense_block_scaling: float32 [2048], replicated, may hold values from 0.1 to 1.9
- widen_projection_weights: bfloat16 [2048, 8192], P('sp', 'tp'), may hold values from -0.125 to 0.125
- shrink_projection_weights: bfloat16 [8192, 2048], P('tp', 'sp'), may hold values from -0.0625 to 0.0625
Outputs:
- result: bfloat16 [2048, 2048], P('sp', 'tp')
Inputs may be any that keep to these rules, and one draw needn't show every extreme that they name: `sample_membership`: document numbers never fall along the positions; each document holds 1 to 1024 positions.
All inputs are finite; a program needn't handle non-finite values.
Results may differ from a plain program's by a relative error of at most 0.015.
Values may be sent and summed in bfloat16 or wider, within the bound.
A program may use at most 128 MiB of HBM per device.

v0:
```python
import jax
import jax.numpy as jnp
from jax import lax
from jax.sharding import PartitionSpec as P

BLOCK = 64
HIGH = lax.Precision.HIGHEST
EPSILON = 1e-06


def entering(array, axis, combine, identity, reverse):
    length, here = (lax.axis_size(axis), lax.axis_index(axis))
    everything = jax.tree.map(
        lambda part, kind: lax.all_gather(part.astype(kind), axis),
        array,
        jax.tree.map(lambda a: jnp.bfloat16 if a.dtype == jnp.float32 else a.dtype, array),
    )
    start = jax.tree.map(
        lambda part, zero: jnp.broadcast_to(jnp.asarray(zero, part.dtype), part.shape),
        array,
        identity,
    )

    def hop(k, before):
        at = length - 1 - k if reverse else k
        reached = at > here if reverse else at < here
        new = combine(
            before, jax.tree.map(lambda part, own: part[at].astype(own.dtype), everything, array)
        )
        return jax.tree.map(lambda a, b: jnp.where(reached, a, b), new, before)

    return lax.fori_loop(0, length, hop, start)


def block_pass(
    memory,
    probe_vectors,
    lookup_vectors,
    payload_vectors,
    strengths,
    forget_multipliers,
    doc_ids,
    prior_doc,
    wanted,
):
    value_width = payload_vectors.shape[-1]
    block_len = probe_vectors.shape[1]
    running = jnp.cumsum(forget_multipliers, axis=-1)
    row_ids = lax.broadcasted_iota(jnp.int32, (block_len, block_len), 0)
    col_ids = lax.broadcasted_iota(jnp.int32, (block_len, block_len), 1)
    shared = doc_ids[:, None] == doc_ids[None, :]
    within = (row_ids >= col_ids) & shared
    before = (row_ids > col_ids) & shared
    spread = jnp.exp(jnp.where(within, running[:, :, None] - running[:, None, :], -jnp.inf))
    linked = (doc_ids == prior_doc).astype(jnp.float32)
    ending = (doc_ids == doc_ids[-1]).astype(jnp.float32)
    weighted = lookup_vectors * strengths[..., None]
    system = jnp.eye(block_len, dtype=jnp.float32) + jnp.where(
        before, jnp.einsum("hik,hjk->hij", weighted, lookup_vectors, precision=HIGH) * spread, 0.0
    )
    right_side = jnp.concatenate(
        [payload_vectors * strengths[..., None], weighted * (jnp.exp(running) * linked)[..., None]],
        axis=-1,
    )
    solved = jax.scipy.linalg.solve_triangular(system, right_side, lower=True, unit_diagonal=True)
    update = solved[..., :value_width] - jnp.einsum(
        "hck,hkw->hcw", solved[..., value_width:], memory, precision=HIGH
    )
    faded_keys = lookup_vectors * (jnp.exp(running[:, -1:] - running) * ending)[..., None]
    kept_share = jnp.exp(running[:, -1]) * linked[-1]
    renewed = memory * kept_share[:, None, None] + jnp.einsum(
        "hck,hcw->hkw", faded_keys, update, precision=HIGH
    )
    if not wanted:
        return (renewed, None)
    scores = jnp.where(
        within,
        jnp.einsum("hik,hjk->hij", probe_vectors, lookup_vectors, precision=HIGH) * spread,
        0.0,
    )
    reading = jnp.einsum(
        "hck,hkw->hcw",
        probe_vectors * (jnp.exp(running) * linked)[..., None],
        memory,
        precision=HIGH,
    )
    return (renewed, reading + jnp.einsum("hij,hjw->hiw", scores, update, precision=HIGH))


def run_blocks(
    memory,
    prior_doc,
    probe_vectors,
    lookup_vectors,
    payload_vectors,
    strengths,
    forget_multipliers,
    doc_ids,
    wanted,
):
    head_count, length, key_width = probe_vectors.shape
    block_count = length // BLOCK

    def split_blocks(tensor):
        return jnp.moveaxis(
            tensor.reshape((head_count, block_count, BLOCK) + tensor.shape[2:]), 1, 0
        )

    def advance(carried, inputs):
        held, earlier_doc = carried
        query_block, key_block, value_block, gate_block, decay_block, doc_block = inputs
        held, produced = block_pass(
            held,
            query_block,
            key_block,
            value_block,
            gate_block,
            decay_block,
            doc_block,
            earlier_doc,
            wanted,
        )
        return ((held, doc_block[-1]), produced)

    (final, _), produced = lax.scan(
        advance,
        (memory, prior_doc),
        (
            split_blocks(probe_vectors),
            split_blocks(lookup_vectors),
            split_blocks(payload_vectors),
            split_blocks(strengths),
            split_blocks(forget_multipliers),
            doc_ids.reshape(block_count, BLOCK),
        ),
    )
    if wanted:
        produced = jnp.moveaxis(produced, 0, 1).reshape(head_count, length, -1)
    return (final, produced)


def unit_rows(tensor):
    return tensor * lax.rsqrt(jnp.sum(tensor * tensor, axis=-1, keepdims=True) + EPSILON)


def heads_first(tensor, head_width):
    row_count = tensor.shape[0]
    return jnp.transpose(tensor.astype(jnp.float32).reshape(row_count, -1, head_width), (1, 0, 2))


def summarize(
    probe_vectors, lookup_vectors, payload_vectors, strengths, forget_multipliers, doc_ids
):
    head_count, length, key_width = probe_vectors.shape
    start_map = jnp.concatenate(
        [
            jnp.broadcast_to(
                jnp.eye(key_width, dtype=jnp.float32), (head_count, key_width, key_width)
            ),
            jnp.zeros((head_count, key_width, payload_vectors.shape[-1]), jnp.float32),
        ],
        axis=-1,
    )
    padded = jnp.concatenate(
        [jnp.zeros((head_count, length, key_width), jnp.float32), payload_vectors], axis=-1
    )
    final, _ = run_blocks(
        start_map,
        doc_ids[0],
        probe_vectors,
        lookup_vectors,
        padded,
        strengths,
        forget_multipliers,
        doc_ids,
        False,
    )
    as_float = doc_ids.astype(jnp.float32)
    return (final[..., :key_width], final[..., key_width:], as_float[0], as_float[-1])


def compose(earlier, later):
    early_map, early_shift, early_first, early_last = earlier
    late_map, late_shift, late_first, late_last = later
    joined = ((late_first == early_last) | (early_last < 0) | (late_first < 0)).astype(jnp.float32)
    new_map = jnp.einsum("hij,hjk->hik", late_map, early_map, precision=HIGH) * joined
    new_shift = (
        jnp.einsum("hij,hjk->hik", late_map, early_shift, precision=HIGH) * joined + late_shift
    )
    return (
        new_map,
        new_shift,
        jnp.where(early_first < 0, late_first, early_first),
        jnp.where(late_last < 0, early_last, late_last),
    )


def neutral(head_count, key_width, value_width):
    return (
        jnp.broadcast_to(jnp.eye(key_width, dtype=jnp.float32), (head_count, key_width, key_width)),
        jnp.zeros((head_count, key_width, value_width), jnp.float32),
        jnp.full((), -1.0, jnp.float32),
        jnp.full((), -1.0, jnp.float32),
    )


def shards(
    skip_path_inputs,
    probe_vectors,
    lookup_vectors,
    payload_vectors,
    learning_strength_preacts,
    forget_preacts,
    forgetting_speed_exponent,
    extra_forgetting_spikes,
    sample_membership,
    channel_group_scaling,
    blend_exit_weights,
    dense_block_scaling,
    widen_projection_weights,
    shrink_projection_weights,
):
    length = probe_vectors.shape[0]
    key_width = channel_group_scaling.shape[0]
    query_heads = unit_rows(heads_first(probe_vectors, key_width)) * key_width ** (-0.5)
    key_heads = unit_rows(heads_first(lookup_vectors, key_width))
    value_heads = heads_first(payload_vectors, key_width)
    head_count = query_heads.shape[0]
    strengths = jnp.transpose(jax.nn.sigmoid(learning_strength_preacts), (0, 2, 1))
    forget_multipliers = jnp.transpose(
        -jnp.exp(forgetting_speed_exponent)[:, None, :] * jax.nn.softplus(forget_preacts)
        + extra_forgetting_spikes,
        (0, 2, 1),
    )
    forward_parts = summarize(
        query_heads, key_heads, value_heads, strengths[0], forget_multipliers[0], sample_membership
    )
    forward_prefix = entering(
        forward_parts, "sp", compose, neutral(head_count, key_width, key_width), False
    )
    _, forward_out = run_blocks(
        forward_prefix[1],
        forward_prefix[3].astype(jnp.int32),
        query_heads,
        key_heads,
        value_heads,
        strengths[0],
        forget_multipliers[0],
        sample_membership,
        True,
    )
    flipped_queries = jnp.flip(query_heads, 1)
    flipped_keys = jnp.flip(key_heads, 1)
    flipped_values = jnp.flip(value_heads, 1)
    flipped_gates = jnp.flip(strengths[1], 1)
    flipped_decays = jnp.flip(forget_multipliers[1], 1)
    flipped_docs = jnp.flip(sample_membership, 0)
    backward_parts = summarize(
        flipped_queries, flipped_keys, flipped_values, flipped_gates, flipped_decays, flipped_docs
    )
    backward_prefix = entering(
        backward_parts, "sp", compose, neutral(head_count, key_width, key_width), True
    )
    _, backward_out = run_blocks(
        backward_prefix[1],
        backward_prefix[3].astype(jnp.int32),
        flipped_queries,
        flipped_keys,
        flipped_values,
        flipped_gates,
        flipped_decays,
        flipped_docs,
        True,
    )
    attn = forward_out + jnp.flip(backward_out, 1)
    scaled = (
        attn
        * lax.rsqrt(jnp.mean(attn * attn, axis=-1, keepdims=True) + EPSILON)
        * channel_group_scaling
    )
    mixed = (
        jnp.transpose(scaled, (1, 0, 2))
        .reshape(length, head_count * key_width)
        .astype(jnp.bfloat16)
    )
    head_terms = lax.optimization_barrier(
        jnp.dot(mixed, blend_exit_weights, preferred_element_type=jnp.float32).astype(jnp.bfloat16)
    ).astype(jnp.float32)
    model_width = skip_path_inputs.shape[1]
    col_count = model_width // lax.axis_size("tp")
    col_start = lax.axis_index("tp") * col_count
    summed = lax.psum(head_terms.astype(jnp.bfloat16), "tp").astype(jnp.float32)
    residual = skip_path_inputs.astype(jnp.float32) + summed
    normed = (
        residual
        * lax.rsqrt(jnp.mean(residual * residual, axis=1, keepdims=True) + EPSILON)
        * dense_block_scaling
    ).astype(jnp.bfloat16)
    own_residual = lax.dynamic_slice_in_dim(residual, col_start, col_count, 1)
    raised = jnp.dot(
        normed,
        lax.all_gather(widen_projection_weights, "sp", axis=0, tiled=True),
        preferred_element_type=jnp.float32,
    )
    active = jnp.square(jax.nn.relu(raised)).astype(jnp.bfloat16)
    lowered = jnp.dot(
        active,
        lax.all_gather(shrink_projection_weights, "sp", axis=1, tiled=True),
        preferred_element_type=jnp.float32,
    )
    rounded = lax.optimization_barrier(lowered.astype(jnp.bfloat16)).astype(jnp.float32)
    mixer_cols = lax.psum_scatter(
        rounded.astype(jnp.bfloat16), "tp", scatter_dimension=1, tiled=True
    ).astype(jnp.float32)
    return (own_residual + mixer_cols).astype(jnp.bfloat16)


def solution(mesh):
    placed = (
        P("sp", None),
        P("sp", "tp"),
        P("sp", "tp"),
        P("sp", "tp"),
        P(None, "sp", "tp"),
        P(None, "sp", "tp"),
        P(None, "tp"),
        P(None, "sp", "tp"),
        P("sp"),
        P(),
        P("tp", None),
        P(),
        P("sp", "tp"),
        P("tp", "sp"),
    )
    return jax.shard_map(
        shards, mesh=mesh, in_specs=placed, out_specs=P("sp", "tp"), check_vma=False
    )
```

profile of v0, /device:TPU:0, one launch (start us, length us, event | category | flops | bytes accessed | tf_op | source)
XLA Modules:
  0.0 1001.6 jit_solution(841433032563091980)
XLA Ops:
  15.5 1.8 concatenate.24.clone
  17.3 59.1 %while.88 = (s32[]{:T(128)}, f32[4,128,256]{2,1,0:T(8,128)S(1)}, s32[]{:T(128)}, f32[2,4,64]{2,1,0:T(4,128)}, s32[2,64]{1,0:T(2,128)}, /*index=5*/f32[2,4,64,128...) while((s32[]{:T(128)}, f32[4,128,256]{2,1,0:T(8,128)S(1)}, ...), condition=%wide.region_12.15_spmd, body=%wide.region_10.14_spmd.sunk | while | flops 302785408 | bytes 4747572 | solution.py:125
  20.7 20.4 %custom-call.20 = f32[4,1,64,64]{2,3,1,0:T(8,128)S(1)} custom-call(f32[4,1,64,64]{3,2,1,0:T(8,128)} %fusion.286), custom_call_target="InvertDiagBlocksLowerTriangular" | custom-call | tf_op jit(solution)/shard_map/while/body/eval_jaxpr/jit(_solve_triangular)/vmap()/triangular_solve | solution.py:65
  50.2 20.4 %custom-call.20 = f32[4,1,64,64]{2,3,1,0:T(8,128)S(1)} custom-call(f32[4,1,64,64]{3,2,1,0:T(8,128)} %fusion.286), custom_call_target="InvertDiagBlocksLowerTriangular" | custom-call | tf_op jit(solution)/shard_map/while/body/eval_jaxpr/jit(_solve_triangular)/vmap()/triangular_solve | solution.py:65
  78.1 1.8 copy.86
  84.8 59.3 %while.86 = (s32[]{:T(128)}, f32[4,128,256]{2,1,0:T(8,128)S(1)}, s32[]{:T(128)}, f32[2,4,64]{2,1,0:T(4,128)}, s32[2,64]{1,0:T(2,128)}, /*index=5*/f32[2,4,64,128...) while((s32[]{:T(128)}, f32[4,128,256]{2,1,0:T(8,128)S(1)}, ...), condition=%wide.region_3.5_spmd, body=%wide.region_1.4_spmd.sunk | while | flops 302785408 | bytes 4747572 | solution.py:125
  88.2 20.4 %custom-call.18 = f32[4,1,64,64]{2,3,1,0:T(8,128)S(1)} custom-call(f32[4,1,64,64]{3,2,1,0:T(8,128)} %fusion.256), custom_call_target="InvertDiagBlocksLowerTriangular" | custom-call | tf_op jit(solution)/shard_map/while/body/eval_jaxpr/jit(_solve_triangular)/vmap()/triangular_solve | solution.py:65
  117.8 20.4 %custom-call.18 = f32[4,1,64,64]{2,3,1,0:T(8,128)S(1)} custom-call(f32[4,1,64,64]{3,2,1,0:T(8,128)} %fusion.256), custom_call_target="InvertDiagBlocksLowerTriangular" | custom-call | tf_op jit(solution)/shard_map/while/body/eval_jaxpr/jit(_solve_triangular)/vmap()/triangular_solve | solution.py:65
  149.9 1.9 reverse.4
  152.6 1.8 copy.109
  155.1 1.4 dynamic-update-slice.2
  156.5 1.5 dynamic-update-slice.3
  158.0 1.4 dynamic-update-slice
  160.7 1.8 copy.95
  162.5 45.0 %all-reduce.7 = (bf16[16]{0:T(256)(128)(2,1)S(1)}, bf16[16]{0:T(256)(128)(2,1)S(1)}, bf16[16]{0:T(256)(128)(2,1)}, bf16[16]{0:T(256)(128)(2,1)}) all-reduce(bf16[16]{0:T(256)(128)(2,1)S(1)} %dynamic-update-slice.2, bf16[16]{0:T(256)(128)(2,1)S(1)} %dynamic-update-slice.3, ...), channel_id=1, replica_groups=mesh['sp'=16,'tp'=2] {'sp'}, use_global_device_ids=true, to_apply=%add.5 | all-reduce | flops 64 | bytes 256
  207.5 74.9 %while.91 = (s32[]{:T(128)}, f32[4,128,128]{2,1,0:T(8,128)S(1)}, f32[]{:T(128)}, s32[]{:T(128)}, bf16[16,4,128,128]{3,2,1,0:T(8,128)(2,1)}, /*index=5*/bf16[16]{...) while((s32[]{:T(128)}, f32[4,128,128]{2,1,0:T(8,128)S(1)}, ...), condition=%wide.region_14.17_spmd.clone, body=%wide.region_13.16_spmd.clone.sunk | while | flops 101056528 | bytes 1576206 | solution.py:32
  283.2 60.2 %while.89 = (s32[]{:T(128)}, f32[4,128,128]{2,1,0:T(8,128)S(1)}, s32[]{:T(128)}, f32[2,4,64,128]{3,2,0,1:T(8,128)}, f32[2,4,64]{2,1,0:T(4,128)}, /*index=5*/s32[...) while((s32[]{:T(128)}, f32[4,128,128]{2,1,0:T(8,128)S(1)}, ...), condition=%wide.region_17.20_spmd, body=%wide.region_15.19_spmd.sunk | while | flops 277521280 | bytes 7515824 | solution.py:125
  285.8 19.7 %custom-call.21 = f32[4,1,64,64]{2,3,1,0:T(8,128)S(1)} custom-call(f32[4,1,64,64]{3,2,1,0:T(8,128)S(1)} %fusion.302), custom_call_target="InvertDiagBlocksLowerTriangular" | custom-call | tf_op jit(solution)/shard_map/while/body/eval_jaxpr/jit(_solve_triangular)/vmap()/triangular_solve | solution.py:65
  315.9 19.7 %custom-call.21 = f32[4,1,64,64]{2,3,1,0:T(8,128)S(1)} custom-call(f32[4,1,64,64]{3,2,1,0:T(8,128)S(1)} %fusion.302), custom_call_target="InvertDiagBlocksLowerTriangular" | custom-call | tf_op jit(solution)/shard_map/while/body/eval_jaxpr/jit(_solve_triangular)/vmap()/triangular_solve | solution.py:65
  343.4 3.0 rev.30
  346.3 103.0 %while.90 = (s32[]{:T(128)}, f32[4,128,128]{2,1,0:T(8,128)S(1)}, f32[]{:T(128)}, s32[]{:T(128)}, bf16[16,4,128,128]{3,2,1,0:T(8,128)(2,1)}, /*index=5*/bf16[16]{...) while((s32[]{:T(128)}, f32[4,128,128]{2,1,0:T(8,128)S(1)}, ...), condition=%wide.region_5.7_spmd.clone, body=%wide.region_4.6_spmd.clone.sunk | while | flops 101056520 | bytes 1576144 | solution.py:32
  346.4 1.4 dynamic_slice.315
  450.1 56.9 %while.87 = (s32[]{:T(128)}, f32[4,128,128]{2,1,0:T(8,128)S(1)}, s32[]{:T(128)}, f32[2,4,64,128]{3,2,0,1:T(8,128)}, f32[2,4,64]{2,1,0:T(4,128)}, /*index=5*/s32[...) while((s32[]{:T(128)}, f32[4,128,128]{2,1,0:T(8,128)S(1)}, ...), condition=%wide.region_9.12_spmd, body=%wide.region_7.11_spmd.sunk | while | flops 277521280 | bytes 6467220 | solution.py:125
  452.7 19.7 %custom-call.19 = f32[4,1,64,64]{2,3,1,0:T(8,128)S(1)} custom-call(f32[4,1,64,64]{3,2,1,0:T(8,128)S(1)} %fusion.272), custom_call_target="InvertDiagBlocksLowerTriangular" | custom-call | tf_op jit(solution)/shard_map/while/body/eval_jaxpr/jit(_solve_triangular)/vmap()/triangular_solve | solution.py:65
  481.2 19.7 %custom-call.19 = f32[4,1,64,64]{2,3,1,0:T(8,128)S(1)} custom-call(f32[4,1,64,64]{3,2,1,0:T(8,128)S(1)} %fusion.272), custom_call_target="InvertDiagBlocksLowerTriangular" | custom-call | tf_op jit(solution)/shard_map/while/body/eval_jaxpr/jit(_solve_triangular)/vmap()/triangular_solve | solution.py:65
  512.5 13.0 %all-reduce.10.cloned.1.call-done = bf16[128,2048]{1,0:T(8,128)(2,1)} async-done(((bf16[128,2048]{1,0:T(8,128)(2,1)}), bf16[128,2048]{1,0:T(8,128)(2,1)}) %all-reduce.10.cloned.1.call-update) | async-done | bytes 524304 | tf_op jit(solution)/shard_map/psum | solution.py:292
  525.5 1.5 convert_add_fusion
  526.9 193.4 %all-gather.11.cloned.1.call-done = bf16[2048,4096]{1,0:T(8,128)(2,1)} async-done(((bf16[128,4096]{1,0:T(8,128)(2,1)}), bf16[2048,4096]{1,0:T(8,128)(2,1)}) %all-gather.11.cloned.1.call-update) | async-done | bytes 16777232 | tf_op jit(solution)/shard_map/all_gather | solution.py:302
  720.3 250.0 %all-gather.13.cloned.1.call-done = bf16[4096,2048]{1,0:T(8,128)(2,1)} async-done(((bf16[4096,128]{1,0:T(8,128)(2,1)}), bf16[4096,2048]{1,0:T(8,128)(2,1)}) %all-gather.13.cloned.1.call-update) | async-done | bytes 16777232 | tf_op jit(solution)/shard_map/all_gather | solution.py:308
  970.4 16.4 %convolution_convert_fusion = bf16[128,2048]{1,0:T(8,128)(2,1)} fusion(bf16[4096,2048]{1,0:T(8,128)(2,1)} %all-gather.13.cloned.1.call-done, bf16[2048,4096]{1,0:T(8,128)(2,1)} %all-gather.11.cloned.1.call-done, f32[2048]{0:T(1024)S(1)} %copy-done.16, f32[128]{0:T(128)S(1)} %add_rsqrt_fusion.3, bf16[128,2048]{1,0:T(8,128)(2,1)} %all-reduce.10.cloned.1.call-done, ...), kind=kOutput, calls=%fused_computation.245 | convolution fusion | flops 4298375168 | bytes 35136000 | tf_op jit(solution)/shard_map/dot_general | solution.py:306
  986.8 6.3 reduce-scatter.2.cloned.1.call-done
  993.0 1.7 add_convert_fusion
  (427 shorter events, 194.3 us)
Async XLA Ops:
  6.5 503.0 %copy-start = (bf16[512,2048]{1,0:T(8,128)(2,1)S(1)}, bf16[512,2048]{1,0:T(8,128)(2,1)}, u32[]{:S(2)}) copy-start(bf16[512,2048]{1,0:T(8,128)(2,1)} %param.40) | copy-start | bytes 6291460
  6.5 4.0 copy-start.11
  6.5 5.4 copy-start.21
  6.5 5.4 copy-start.18
  6.5 5.4 copy-start.17
  6.5 6.8 copy-start.19
  6.6 201.0 %all-gather.19.cloned.1.call-start = ((), (), s32[]{:S(2)}) async-start(), calls=%async_computation.7 | async-start | bytes 2228224 | tf_op jit(solution)/shard_map/all_gather | solution.py:14
  7.5 7.9 copy-start.23
  10.0 5.4 copy-start.5
  10.7 4.7 copy-start.6
  76.4 4.5 copy-start.20
  76.4 6.1 copy-start.14
  76.4 6.8 copy-start.15
  77.3 130.3 %all-gather.21.cloned.1.call-start = ((), (), s32[]{:S(2)}) async-start(), calls=%async_computation.8 | async-start | bytes 2228224 | tf_op jit(solution)/shard_map/all_gather | solution.py:14
  78.0 268.3 %all-gather.15.cloned.1.call-start = ((), (), s32[]{:S(2)}) async-start(), calls=%async_computation.5 | async-start | bytes 2228224 | tf_op jit(solution)/shard_map/all_gather | solution.py:14
  80.9 3.8 copy-start.3
  144.1 10.4 %copy-start.22 = (u32[32]{0:T(128)S(1)}, u32[32]{0:T(128)}, u32[]{:S(2)}) copy-start(u32[32]{0:T(128)} %constant.207) | copy-start | bytes 388
  144.9 201.4 %all-gather.17.cloned.1.call-start = ((), (), s32[]{:S(2)}) async-start(), calls=%async_computation.6 | async-start | bytes 2228224 | tf_op jit(solution)/shard_map/all_gather | solution.py:14
  145.5 380.0 %all-reduce.10.cloned.1.call-start = ((), (), s32[]{:S(2)}) async-start(), calls=%async_computation.1 | async-start | bytes 1048576 | tf_op jit(solution)/shard_map/psum | solution.py:292
  305.5 4.9 copy-start.2
  305.5 4.9 copy-start.9
  305.5 5.3 copy-start.12
  335.5 4.9 copy-start.2
  335.6 4.9 copy-start.9
  335.6 5.3 copy-start.12
  346.3 103.8 %copy-start.1 = (f32[4,128,128]{2,1,0:T(8,128)S(1)}, f32[4,128,128]{2,1,0:T(8,128)}, u32[]{:S(2)}) copy-start(f32[4,128,128]{2,1,0:T(8,128)} %copy.95) | copy-start | bytes 786436
  346.3 103.8 %copy-start.4 = (f32[4,128,128]{2,1,0:T(8,128)S(1)}, f32[4,128,128]{2,1,0:T(8,128)}, u32[]{:S(2)}) copy-start(f32[4,128,128]{2,1,0:T(8,128)} %copy-done.3) | copy-start | bytes 786436
  500.9 3.5 copy-start.13
  510.8 459.5 %copy-start.16 = (f32[2048]{0:T(1024)S(1)}, f32[2048]{0:T(1024)}, u32[]{:S(2)}) copy-start(f32[2048]{0:T(1024)} %param.41) | copy-start | bytes 24580
  510.9 209.5 %all-gather.11.cloned.1.call-start = ((), (), s32[]{:S(2)}) async-start(), calls=%async_computation.2 | async-start | bytes 17825792 | tf_op jit(solution)/shard_map/all_gather | solution.py:302
  511.4 458.9 %all-gather.13.cloned.1.call-start = ((), (), s32[]{:S(2)}) async-start(), calls=%async_computation.3 | async-start | bytes 17825792 | tf_op jit(solution)/shard_map/all_gather | solution.py:308
  512.2 480.8 %reduce-scatter.2.cloned.1.call-start = ((), (), s32[]{:S(2)}) async-start(), calls=%async_computation.4 | async-start | bytes 786432 | tf_op jit(solution)/shard_map/reduce_scatter | solution.py:312
  (7 other events, 14.6 us)
Sparse Core Ops, SparseCore 0:
  77.4 64.2 all-gather.18
  144.4 59.3 all-gather.20
  206.6 59.2 all-gather.14
  268.4 60.8 all-gather.16
  511.0 14.4 all-reduce.9
  528.1 192.1 all-gather.10
  723.0 247.2 all-gather.12
  986.9 6.0 reduce-scatter.1
where the time goes:
time: 1010 us; the launch traced here: 1000 us
  waiting for transfers between devices  465 us (46%)
  other arithmetic  192 us (19%)
  local copies, waits for them, and re-layouts  114 us (11%)
  loops' own time  88.3 us (9%)
  matrix products  82.7 us (8%)
  blocking collectives  45 us (4%)
  between operations  13.9 us (1%)
    all_gather x1, waiting for transfers between devices, shards(): lax.all_gather(shrink_projection_weights, 'sp', axis=1, tiled=True)  250 us
    all_gather x1, waiting for transfers between devices, shards(): lax.all_gather(widen_projection_weights, 'sp', axis=0, tiled=True)  193 us
    another operation x16, other arithmetic, block_pass(): jax.scipy.linalg.solve_triangular(system, right_side, lower=True, unit_di...  160 us
    another operation x2, loops' own time, entering(): return lax.fori_loop(0, length, hop, start)  77.3 us
    dynamic_slice x64, local copies, waits for them, and re-layouts, hop(): part[at].astype(own.dtype)  59.4 us
    unnamed x1, blocking collectives  45 us
    dot_general x32, matrix products, compose(): jnp.einsum('hij,hjk->hik', late_map, early_shift, precision=HIGH) * joined  40.6 us
  transfers between devices with their start and end apart: 8, of which 4 were waited for; matrix products, arithmetic and copies ran while one was open for 18% of the time, Pallas kernels for 0%

commit v1 on v0

--- a/solution.py
+++ b/solution.py
@@ -305,7 +305,7 @@
     active = jnp.square(jax.nn.relu(raised)).astype(jnp.bfloat16)
     lowered = jnp.dot(
         active,
-        lax.all_gather(shrink_projection_weights, "sp", axis=1, tiled=True),
+        jnp.concatenate(lax.all_gather(shrink_projection_weights, "sp"), axis=1),
         preferred_element_type=jnp.float32,
     )
     rounded = lax.optimization_barrier(lowered.astype(jnp.bfloat16)).astype(jnp.float32)

time: 1010 us -> 947 us (0.938)
  waiting for transfers between devices: 465 us -> 386 us
  local copies, waits for them, and re-layouts: 114 us -> 136 us
    all_gather x1, waiting for transfers between devices: 250 us -> 193 us  [shards(): lax.all_gather(shrink_projection_weights, 'sp')]
    all_gather x1, waiting for transfers between devices: 193 us -> 170 us  [shards(): lax.all_gather(widen_projection_weights, 'sp', axis=0, tiled=True)]
    reshape x0 -> x1, local copies, waits for them, and re-layouts: none -> 21.6 us  [shards(): jnp.concatenate(lax.all_gather(shrink_projection_weights, 'sp'), axis=1)]
  transfers between devices with their start and end apart: 8 -> 8, of which waited for: 4 -> 4; matrix products, arithmetic and copies ran while one was open for 18% -> 22% of each run, Pallas kernels for 0% -> 0%
where the time goes in v1:
time: 947 us; the launch traced here: 943 us
  waiting for transfers between devices  386 us (41%)
  other arithmetic  192 us (20%)
  local copies, waits for them, and re-layouts  136 us (14%)
  loops' own time  88.3 us (9%)
  matrix products  82.2 us (9%)
  blocking collectives  45 us (5%)
  between operations  13.8 us (1%)
    all_gather x1, waiting for transfers between devices, shards(): lax.all_gather(shrink_projection_weights, 'sp')  193 us
    all_gather x1, waiting for transfers between devices, shards(): lax.all_gather(widen_projection_weights, 'sp', axis=0, tiled=True)  170 us
    another operation x16, other arithmetic, block_pass(): jax.scipy.linalg.solve_triangular(system, right_side, lower=True, unit_di...  160 us
    another operation x2, loops' own time, entering(): return lax.fori_loop(0, length, hop, start)  77.3 us
    dynamic_slice x64, local copies, waits for them, and re-layouts, hop(): part[at].astype(own.dtype)  59.4 us
    unnamed x1, blocking collectives  45 us
    dot_general x32, matrix products, compose(): jnp.einsum('hij,hjk->hik', late_map, early_shift, precision=HIGH) * joined  40.6 us
    reshape x1, local copies, waits for them, and re-layouts, shards(): jnp.concatenate(lax.all_gather(shrink_projection_weights, 'sp'), axis=1)  21.6 us
  transfers between devices with their start and end apart: 8, of which 4 were waited for; matrix products, arithmetic and copies ran while one was open for 22% of the time, Pallas kernels for 0%

profile of v1, /device:TPU:0, one launch (start us, length us, event | category | flops | bytes accessed | tf_op | source)
XLA Modules:
  0.0 943.0 jit_solution(17626101829487198396)
XLA Ops:
  15.5 1.8 concatenate.24.clone
  17.3 59.1 %while.88 = (s32[]{:T(128)}, f32[4,128,256]{2,1,0:T(8,128)S(1)}, s32[]{:T(128)}, f32[2,4,64]{2,1,0:T(4,128)}, s32[2,64]{1,0:T(2,128)}, /*index=5*/f32[2,4,64,128...) while((s32[]{:T(128)}, f32[4,128,256]{2,1,0:T(8,128)S(1)}, ...), condition=%wide.region_12.15_spmd, body=%wide.region_10.14_spmd.sunk | while | flops 302785408 | bytes 4747572 | solution.py:125
  20.7 20.4 %custom-call.20 = f32[4,1,64,64]{2,3,1,0:T(8,128)S(1)} custom-call(f32[4,1,64,64]{3,2,1,0:T(8,128)} %fusion.286), custom_call_target="InvertDiagBlocksLowerTriangular" | custom-call | tf_op jit(solution)/shard_map/while/body/eval_jaxpr/jit(_solve_triangular)/vmap()/triangular_solve | solution.py:65
  50.2 20.4 %custom-call.20 = f32[4,1,64,64]{2,3,1,0:T(8,128)S(1)} custom-call(f32[4,1,64,64]{3,2,1,0:T(8,128)} %fusion.286), custom_call_target="InvertDiagBlocksLowerTriangular" | custom-call | tf_op jit(solution)/shard_map/while/body/eval_jaxpr/jit(_solve_triangular)/vmap()/triangular_solve | solution.py:65
  78.1 1.8 copy.87
  84.8 59.3 %while.86 = (s32[]{:T(128)}, f32[4,128,256]{2,1,0:T(8,128)S(1)}, s32[]{:T(128)}, f32[2,4,64]{2,1,0:T(4,128)}, s32[2,64]{1,0:T(2,128)}, /*index=5*/f32[2,4,64,128...) while((s32[]{:T(128)}, f32[4,128,256]{2,1,0:T(8,128)S(1)}, ...), condition=%wide.region_3.5_spmd, body=%wide.region_1.4_spmd.sunk | while | flops 302785408 | bytes 4747572 | solution.py:125
  88.2 20.4 %custom-call.18 = f32[4,1,64,64]{2,3,1,0:T(8,128)S(1)} custom-call(f32[4,1,64,64]{3,2,1,0:T(8,128)} %fusion.256), custom_call_target="InvertDiagBlocksLowerTriangular" | custom-call | tf_op jit(solution)/shard_map/while/body/eval_jaxpr/jit(_solve_triangular)/vmap()/triangular_solve | solution.py:65
  117.8 20.4 %custom-call.18 = f32[4,1,64,64]{2,3,1,0:T(8,128)S(1)} custom-call(f32[4,1,64,64]{3,2,1,0:T(8,128)} %fusion.256), custom_call_target="InvertDiagBlocksLowerTriangular" | custom-call | tf_op jit(solution)/shard_map/while/body/eval_jaxpr/jit(_solve_triangular)/vmap()/triangular_solve | solution.py:65
  149.9 1.9 reverse.4
  152.6 1.8 copy.110
  155.1 1.4 dynamic-update-slice.2
  156.5 1.5 dynamic-update-slice.3
  158.0 1.4 dynamic-update-slice
  160.7 1.8 copy.96
  162.5 45.0 %all-reduce.7 = (bf16[16]{0:T(256)(128)(2,1)S(1)}, bf16[16]{0:T(256)(128)(2,1)S(1)}, bf16[16]{0:T(256)(128)(2,1)}, bf16[16]{0:T(256)(128)(2,1)}) all-reduce(bf16[16]{0:T(256)(128)(2,1)S(1)} %dynamic-update-slice.2, bf16[16]{0:T(256)(128)(2,1)S(1)} %dynamic-update-slice.3, ...), channel_id=1, replica_groups=mesh['sp'=16,'tp'=2] {'sp'}, use_global_device_ids=true, to_apply=%add.5 | all-reduce | flops 64 | bytes 256
  207.5 74.9 %while.91 = (s32[]{:T(128)}, f32[4,128,128]{2,1,0:T(8,128)S(1)}, f32[]{:T(128)}, s32[]{:T(128)}, bf16[16,4,128,128]{3,2,1,0:T(8,128)(2,1)}, /*index=5*/bf16[16]{...) while((s32[]{:T(128)}, f32[4,128,128]{2,1,0:T(8,128)S(1)}, ...), condition=%wide.region_14.17_spmd.clone, body=%wide.region_13.16_spmd.clone.sunk | while | flops 101056528 | bytes 1576206 | solution.py:32
  283.2 60.2 %while.89 = (s32[]{:T(128)}, f32[4,128,128]{2,1,0:T(8,128)S(1)}, s32[]{:T(128)}, f32[2,4,64,128]{3,2,0,1:T(8,128)}, f32[2,4,64]{2,1,0:T(4,128)}, /*index=5*/s32[...) while((s32[]{:T(128)}, f32[4,128,128]{2,1,0:T(8,128)S(1)}, ...), condition=%wide.region_17.20_spmd, body=%wide.region_15.19_spmd.sunk | while | flops 277521280 | bytes 7515824 | solution.py:125
  285.8 19.7 %custom-call.21 = f32[4,1,64,64]{2,3,1,0:T(8,128)S(1)} custom-call(f32[4,1,64,64]{3,2,1,0:T(8,128)S(1)} %fusion.302), custom_call_target="InvertDiagBlocksLowerTriangular" | custom-call | tf_op jit(solution)/shard_map/while/body/eval_jaxpr/jit(_solve_triangular)/vmap()/triangular_solve | solution.py:65
  315.9 19.7 %custom-call.21 = f32[4,1,64,64]{2,3,1,0:T(8,128)S(1)} custom-call(f32[4,1,64,64]{3,2,1,0:T(8,128)S(1)} %fusion.302), custom_call_target="InvertDiagBlocksLowerTriangular" | custom-call | tf_op jit(solution)/shard_map/while/body/eval_jaxpr/jit(_solve_triangular)/vmap()/triangular_solve | solution.py:65
  343.4 3.0 rev.30
  346.3 103.0 %while.90 = (s32[]{:T(128)}, f32[4,128,128]{2,1,0:T(8,128)S(1)}, f32[]{:T(128)}, s32[]{:T(128)}, bf16[16,4,128,128]{3,2,1,0:T(8,128)(2,1)}, /*index=5*/bf16[16]{...) while((s32[]{:T(128)}, f32[4,128,128]{2,1,0:T(8,128)S(1)}, ...), condition=%wide.region_5.7_spmd.clone, body=%wide.region_4.6_spmd.clone.sunk | while | flops 101056520 | bytes 1576144 | solution.py:32
  450.1 56.9 %while.87 = (s32[]{:T(128)}, f32[4,128,128]{2,1,0:T(8,128)S(1)}, s32[]{:T(128)}, f32[2,4,64,128]{3,2,0,1:T(8,128)}, f32[2,4,64]{2,1,0:T(4,128)}, /*index=5*/s32[...) while((s32[]{:T(128)}, f32[4,128,128]{2,1,0:T(8,128)S(1)}, ...), condition=%wide.region_9.12_spmd, body=%wide.region_7.11_spmd.sunk | while | flops 277521280 | bytes 6467220 | solution.py:125
  452.7 19.7 %custom-call.19 = f32[4,1,64,64]{2,3,1,0:T(8,128)S(1)} custom-call(f32[4,1,64,64]{3,2,1,0:T(8,128)S(1)} %fusion.272), custom_call_target="InvertDiagBlocksLowerTriangular" | custom-call | tf_op jit(solution)/shard_map/while/body/eval_jaxpr/jit(_solve_triangular)/vmap()/triangular_solve | solution.py:65
  481.2 19.7 %custom-call.19 = f32[4,1,64,64]{2,3,1,0:T(8,128)S(1)} custom-call(f32[4,1,64,64]{3,2,1,0:T(8,128)S(1)} %fusion.272), custom_call_target="InvertDiagBlocksLowerTriangular" | custom-call | tf_op jit(solution)/shard_map/while/body/eval_jaxpr/jit(_solve_triangular)/vmap()/triangular_solve | solution.py:65
  512.4 13.0 %all-reduce.10.cloned.1.call-done = bf16[128,2048]{1,0:T(8,128)(2,1)} async-done(((bf16[128,2048]{1,0:T(8,128)(2,1)}), bf16[128,2048]{1,0:T(8,128)(2,1)}) %all-reduce.10.cloned.1.call-update) | async-done | bytes 524304 | tf_op jit(solution)/shard_map/psum | solution.py:292
  525.4 1.5 convert_add_fusion
  526.9 193.4 %all-gather.22.cloned.1.call-done = bf16[65536,128]{1,0:T(8,128)(2,1)} async-done(((bf16[4096,128]{1,0:T(8,128)(2,1)}), bf16[65536,128]{1,0:T(8,128)(2,1)}) %all-gather.22.cloned.1.call-update) | async-done | bytes 16777232 | tf_op jit(solution)/shard_map/all_gather | solution.py:308
  720.3 21.6 %copy.118 = bf16[4096,16,128]{0,2,1:T(8,128)(2,1)} copy(bf16[4096,16,128]{2,0,1:T(8,128)(2,1)} %bitcast.435) | data formatting | bytes 33554432 | tf_op jit(solution)/shard_map/reshape | solution.py:308
  741.9 170.4 %all-gather.12.cloned.1.call-done = bf16[2048,4096]{1,0:T(8,128)(2,1)} async-done(((bf16[128,4096]{1,0:T(8,128)(2,1)}), bf16[2048,4096]{1,0:T(8,128)(2,1)}) %all-gather.12.cloned.1.call-update) | async-done | bytes 16777232 | tf_op jit(solution)/shard_map/all_gather | solution.py:302
  912.3 15.9 %convolution_convert_fusion = bf16[128,2048]{1,0:T(8,128)(2,1)} fusion(bf16[4096,2048]{0,1:T(8,128)(2,1)} %bitcast.434, bf16[2048,4096]{1,0:T(8,128)(2,1)} %all-gather.12.cloned.1.call-done, f32[2048]{0:T(1024)S(1)} %copy-done.16, f32[128]{0:T(128)S(1)} %add_rsqrt_fusion.3, bf16[128,2048]{1,0:T(8,128)(2,1)} %all-reduce.10.cloned.1.call-done, ...), kind=kOutput, calls=%fused_computation.245 | convolution fusion | flops 4298375168 | bytes 35136000 | tf_op jit(solution)/shard_map/dot_general | solution.py:306
  928.2 6.3 reduce-scatter.2.cloned.1.call-done
  934.5 1.7 add_convert_fusion
  (428 shorter events, 195.6 us)
Async XLA Ops:
  6.5 503.0 %copy-start = (bf16[512,2048]{1,0:T(8,128)(2,1)S(1)}, bf16[512,2048]{1,0:T(8,128)(2,1)}, u32[]{:S(2)}) copy-start(bf16[512,2048]{1,0:T(8,128)(2,1)} %param.40) | copy-start | bytes 6291460
  6.5 4.0 copy-start.11
  6.5 5.4 copy-start.21
  6.5 5.4 copy-start.18
  6.5 5.4 copy-start.17
  6.5 6.8 copy-start.19
  6.6 201.0 %all-gather.18.cloned.1.call-start = ((), (), s32[]{:S(2)}) async-start(), calls=%async_computation.6 | async-start | bytes 2228224 | tf_op jit(solution)/shard_map/all_gather | solution.py:14
  7.5 7.9 copy-start.23
  10.0 5.4 copy-start.5
  10.7 4.7 copy-start.6
  76.4 4.5 copy-start.20
  76.4 6.1 copy-start.14
  76.4 6.8 copy-start.15
  77.3 130.3 %all-gather.20.cloned.1.call-start = ((), (), s32[]{:S(2)}) async-start(), calls=%async_computation.7 | async-start | bytes 2228224 | tf_op jit(solution)/shard_map/all_gather | solution.py:14
  78.0 268.3 %all-gather.14.cloned.1.call-start = ((), (), s32[]{:S(2)}) async-start(), calls=%async_computation.4 | async-start | bytes 2228224 | tf_op jit(solution)/shard_map/all_gather | solution.py:14
  80.9 3.8 copy-start.3
  144.1 10.4 %copy-start.22 = (u32[32]{0:T(128)S(1)}, u32[32]{0:T(128)}, u32[]{:S(2)}) copy-start(u32[32]{0:T(128)} %constant.207) | copy-start | bytes 388
  144.9 201.4 %all-gather.16.cloned.1.call-start = ((), (), s32[]{:S(2)}) async-start(), calls=%async_computation.5 | async-start | bytes 2228224 | tf_op jit(solution)/shard_map/all_gather | solution.py:14
  145.5 380.0 %all-reduce.10.cloned.1.call-start = ((), (), s32[]{:S(2)}) async-start(), calls=%async_computation.1 | async-start | bytes 1048576 | tf_op jit(solution)/shard_map/psum | solution.py:292
  305.5 4.9 copy-start.2
  305.5 4.9 copy-start.9
  305.5 5.3 copy-start.12
  335.5 4.9 copy-start.2
  335.6 4.9 copy-start.9
  335.6 5.3 copy-start.12
  346.3 103.8 %copy-start.1 = (f32[4,128,128]{2,1,0:T(8,128)S(1)}, f32[4,128,128]{2,1,0:T(8,128)}, u32[]{:S(2)}) copy-start(f32[4,128,128]{2,1,0:T(8,128)} %copy.96) | copy-start | bytes 786436
  346.3 103.8 %copy-start.4 = (f32[4,128,128]{2,1,0:T(8,128)S(1)}, f32[4,128,128]{2,1,0:T(8,128)}, u32[]{:S(2)}) copy-start(f32[4,128,128]{2,1,0:T(8,128)} %copy-done.3) | copy-start | bytes 786436
  500.9 3.5 copy-start.13
  510.8 209.5 %all-gather.22.cloned.1.call-start = ((), (), s32[]{:S(2)}) async-start(), calls=%async_computation.8 | async-start | bytes 17825792 | tf_op jit(solution)/shard_map/all_gather | solution.py:308
  511.4 400.9 %all-gather.12.cloned.1.call-start = ((), (), s32[]{:S(2)}) async-start(), calls=%async_computation.2 | async-start | bytes 17825792 | tf_op jit(solution)/shard_map/all_gather | solution.py:302
  512.1 422.3 %reduce-scatter.2.cloned.1.call-start = ((), (), s32[]{:S(2)}) async-start(), calls=%async_computation.3 | async-start | bytes 786432 | tf_op jit(solution)/shard_map/reduce_scatter | solution.py:312
  720.3 192.0 %copy-start.16 = (f32[2048]{0:T(1024)S(1)}, f32[2048]{0:T(1024)}, u32[]{:S(2)}) copy-start(f32[2048]{0:T(1024)} %param.41) | copy-start | bytes 24580
  (7 other events, 14.6 us)
Sparse Core Ops, SparseCore 0:
  77.4 64.2 all-gather.17
  144.4 59.3 all-gather.19
  206.6 59.2 all-gather.13
  268.4 60.8 all-gather.15
  510.9 14.4 all-reduce.9
  528.1 192.1 all-gather.21
  723.1 189.1 all-gather.11
  928.4 6.0 reduce-scatter.1
